TPU v7x, 32 devices: a whole 2x2x4 slice. The times are simulated.
32 devices in a mesh: fs: 8 (over z, x), tp: 4 (over y, core).
Axes of the slice: x: 2, y: 2, z: 4, core: 2. Of those that a mesh axis runs over, the one named last changes fastest.
Arguments:
- prompt_rows: bfloat16 [512, 3072], P('tp'), may hold values from -6 to 6
- gate_first: float32 [3072, 8192], P('fs', 'tp'), may hold values from -0.109375 to 0.109375
- up_first: float32 [3072, 8192], P('fs', 'tp'), may hold values from -0.109375 to 0.109375
- down_first: float32 [8192, 3072], P('fs', 'tp'), may hold values from -0.0625 to 0.0625
- gate_second: float32 [3072, 8192], P('fs', 'tp'), may hold values from -0.109375 to 0.109375
- up_second: float32 [3072, 8192], P('fs', 'tp'), may hold values from -0.109375 to 0.109375
- down_second: float32 [8192, 3072], P('fs', 'tp'), may hold values from -0.0625 to 0.0625
- pre_gain_first: float32 [3072], replicated, may hold values from 0.1 to 1.9
- post_gain_first: float32 [3072], replicated, may hold values from 0.1 to 1.9
- pre_gain_second: float32 [3072], replicated, may hold values from 0.1 to 1.9
- post_gain_second: float32 [3072], replicated, may hold values from 0.1 to 1.9
Outputs:
- result_rows: bfloat16 [512, 3072], P('tp')
- gate_first_new: bfloat16 [3072, 8192], P(None, 'fs')
- up_first_new: bfloat16 [3072, 8192], P(None, 'fs')
- down_first_new: bfloat16 [8192, 3072], P('fs')
- gate_second_new: bfloat16 [3072, 8192], P(None, 'fs')
- up_second_new: bfloat16 [3072, 8192], P(None, 'fs')
- down_second_new: bfloat16 [8192, 3072], P('fs')
All inputs are finite; a program needn't handle non-finite values.
Results may differ from a plain program's by a relative error of at most 0.0071.
Values may be sent and summed in bfloat16 or wider, within the bound.
A program may use at most 192 MiB of HBM per device.

v0:
```python
import jax
import jax.numpy as jnp
from jax import lax
from jax.sharding import PartitionSpec as P

EPSILON = 1e-06


def half_step(rows, gate, up, down, post_gain):
    floats = rows.astype(jnp.float32)
    normed = (
        floats * lax.rsqrt(jnp.mean(floats * floats, axis=-1, keepdims=True) + EPSILON)
    ).astype(jnp.bfloat16)
    gate_pre = jnp.dot(normed, gate, preferred_element_type=jnp.float32)
    up_pre = jnp.dot(normed, up, preferred_element_type=jnp.float32)
    hidden = (jax.nn.silu(gate_pre) * up_pre).astype(jnp.bfloat16)
    partial_value = jnp.dot(hidden, down, preferred_element_type=jnp.float32)
    total = lax.psum(partial_value, "fs")
    scale = lax.rsqrt(jnp.mean(total * total, axis=-1, keepdims=True) + EPSILON)
    return (floats + 0.5 * total * scale * post_gain[None, :]).astype(jnp.bfloat16)


def per_device(
    prompt_rows,
    gate_first,
    up_first,
    down_first,
    gate_second,
    up_second,
    down_second,
    pre_gain_first,
    post_gain_first,
    pre_gain_second,
    post_gain_second,
):
    height = gate_first.shape[0]
    start = lax.axis_index("fs") * height
    gain_a = lax.dynamic_slice_in_dim(pre_gain_first, start, height, 0)[:, None]
    gain_b = lax.dynamic_slice_in_dim(pre_gain_second, start, height, 0)[:, None]
    wide = (
        lax.all_gather((gain_a * gate_first).astype(jnp.bfloat16), "tp", axis=1, tiled=True),
        lax.all_gather((gain_a * up_first).astype(jnp.bfloat16), "tp", axis=1, tiled=True),
        lax.all_gather(down_first.astype(jnp.bfloat16), "tp", axis=1, tiled=True),
        lax.all_gather((gain_b * gate_second).astype(jnp.bfloat16), "tp", axis=1, tiled=True),
        lax.all_gather((gain_b * up_second).astype(jnp.bfloat16), "tp", axis=1, tiled=True),
        lax.all_gather(down_second.astype(jnp.bfloat16), "tp", axis=1, tiled=True),
    )
    gate_a, up_a, gate_b, up_b = (
        lax.all_to_all(wide[0], "fs", split_axis=1, concat_axis=0, tiled=True),
        lax.all_to_all(wide[1], "fs", split_axis=1, concat_axis=0, tiled=True),
        lax.all_to_all(wide[3], "fs", split_axis=1, concat_axis=0, tiled=True),
        lax.all_to_all(wide[4], "fs", split_axis=1, concat_axis=0, tiled=True),
    )
    down_a = wide[2]
    down_b = wide[5]
    middle = half_step(prompt_rows, gate_a, up_a, down_a, post_gain_first)
    result = half_step(middle, gate_b, up_b, down_b, post_gain_second)
    return (result, gate_a, up_a, down_a, gate_b, up_b, down_b)


def solution(mesh):
    return jax.shard_map(
        per_device,
        mesh=mesh,
        in_specs=(
            P("tp", None),
            P("fs", "tp"),
            P("fs", "tp"),
            P("fs", "tp"),
            P("fs", "tp"),
            P("fs", "tp"),
            P("fs", "tp"),
            P(),
            P(),
            P(),
            P(),
        ),
        out_specs=(
            P("tp", None),
            P(None, "fs"),
            P(None, "fs"),
            P("fs", None),
            P(None, "fs"),
            P(None, "fs"),
            P("fs", None),
        ),
        check_vma=False,
    )
```

profile of v0, /device:TPU:0, one launch (start us, length us, event | category | flops | bytes accessed | tf_op | source)
XLA Modules:
  0.0 843.3 jit_solution(3647729259422297711)
XLA Ops:
  7.2 0.0 all-gather.7.cloned.1.call-start
  7.2 0.8 dynamic_slice.6
  8.0 5.5 multiply_convert_fusion.3
  13.5 0.0 all-gather.9.cloned.1.call-start
  13.6 0.7 all-gather.9.cloned.1.call-update
  14.3 48.5 %all-gather.7.cloned.1.call-done = bf16[384,8192]{1,0:T(8,128)(2,1)} async-done(((bf16[384,2048]{1,0:T(8,128)(2,1)}), bf16[384,8192]{1,0:T(8,128)(2,1)}) %all-gather.7.cloned.1.call-update) | async-done | bytes 6291472 | tf_op jit(solution)/shard_map/all_gather | solution.py:41
  62.7 6.5 copy.33
  69.2 5.8 all-to-all-start
  75.0 0.0 all-gather.13.cloned.1.call-start
  75.1 0.8 dynamic_slice.7
  75.8 4.5 multiply_convert_fusion.1
  80.4 30.9 %all-gather.9.cloned.1.call-done = bf16[384,8192]{1,0:T(8,128)(2,1)} async-done(((bf16[384,2048]{1,0:T(8,128)(2,1)}), bf16[384,8192]{1,0:T(8,128)(2,1)}) %all-gather.9.cloned.1.call-update) | async-done | bytes 6291472 | tf_op jit(solution)/shard_map/all_gather | solution.py:42
  111.3 6.5 copy.32
  117.8 95.9 %all-to-all-done = bf16[384,8,1024]{2,0,1:T(8,128)(2,1)} async-done(((bf16[384,8,1024]{2,0,1:T(8,128)(2,1)}), bf16[384,8,1024]{2,0,1:T(8,128)(2,1)}, u32[]{:S(2)}, u32[]{:S(2)}) %all-to-all-start) | async-done | bytes 6291488 | tf_op jit(solution)/shard_map/all_to_all | solution.py:49
  213.7 4.8 all-to-all-start.1
  218.4 0.0 all-gather.15.cloned.1.call-start
  218.5 0.5 all-gather.15.cloned.1.call-update
  219.0 6.5 copy.31
  225.5 130.6 %all-to-all-done.1 = bf16[384,8,1024]{2,0,1:T(8,128)(2,1)} async-done(((bf16[384,8,1024]{2,0,1:T(8,128)(2,1)}), bf16[384,8,1024]{2,0,1:T(8,128)(2,1)}, u32[]{:S(2)}, u32[]{:S(2)}) %all-to-all-start.1) | async-done | bytes 6291488 | tf_op jit(solution)/shard_map/all_to_all | solution.py:50
  356.1 4.8 all-to-all-start.2
  361.0 0.0 all-gather.11.cloned.1.call-start
  361.0 3.2 convert_element_type.47
  364.3 0.0 all-reduce.3.cloned.1.call-start
  364.4 0.2 fusion
  364.6 6.5 copy.30
  371.1 4.6 fusion.26
  375.7 35.5 %all-gather.11.cloned.1.call-done = bf16[1024,3072]{1,0:T(8,128)(2,1)} async-done(((bf16[1024,768]{1,0:T(8,128)(2,1)}), bf16[1024,3072]{1,0:T(8,128)(2,1)}) %all-gather.11.cloned.1.call-update) | async-done | bytes 6291472 | tf_op jit(solution)/shard_map/all_gather | solution.py:43
  411.2 7.7 fusion.9
  418.9 100.4 %all-to-all-done.2 = bf16[384,8,1024]{2,0,1:T(8,128)(2,1)} async-done(((bf16[384,8,1024]{2,0,1:T(8,128)(2,1)}), bf16[384,8,1024]{2,0,1:T(8,128)(2,1)}, u32[]{:S(2)}, u32[]{:S(2)}) %all-to-all-start.2) | async-done | bytes 6291488 | tf_op jit(solution)/shard_map/all_to_all | solution.py:51
  519.3 4.8 all-to-all-start.3
  524.1 0.0 all-gather.17.cloned.1.call-start
  524.2 3.3 convert_element_type.54
  527.4 0.2 all-reduce.5.cloned.1.call-start
  527.7 130.8 %all-reduce.3.cloned.1.call-done = f32[128,3072]{1,0:T(8,128)} async-done(((f32[128,3072]{1,0:T(8,128)}), f32[128,3072]{1,0:T(8,128)}) %all-reduce.3.cloned.1.call-update) | async-done | bytes 1572880 | tf_op jit(solution)/shard_map/psum | solution.py:18
  658.5 1.6 multiply_reduce_fusion.1
  660.1 1.9 fusion.3
  662.0 4.2 fusion.22
  666.3 38.0 %all-gather.17.cloned.1.call-done = bf16[1024,3072]{1,0:T(8,128)(2,1)} async-done(((bf16[1024,768]{1,0:T(8,128)(2,1)}), bf16[1024,3072]{1,0:T(8,128)(2,1)}) %all-gather.17.cloned.1.call-update) | async-done | bytes 6291472 | tf_op jit(solution)/shard_map/all_gather | solution.py:46
  704.2 7.7 fusion.8
  712.0 89.4 %all-reduce.5.cloned.1.call-done = f32[128,3072]{1,0:T(8,128)} async-done(((f32[128,3072]{1,0:T(8,128)}), f32[128,3072]{1,0:T(8,128)}) %all-reduce.5.cloned.1.call-update) | async-done | bytes 1572880 | tf_op jit(solution)/shard_map/psum | solution.py:18
  801.4 1.6 multiply_reduce_fusion
  803.0 2.6 fusion.5
  805.6 6.4 copy.42
  812.0 6.3 copy.43
  818.3 2.7 copy.44
  821.0 6.4 copy.45
  827.4 6.3 copy.46
  833.8 2.7 copy.47
  (31 shorter events, 0.2 us)
Async XLA Ops:
  7.2 55.6 %all-gather.7.cloned.1.call-start = ((), (), s32[]{:S(2)}) async-start(), calls=%async_computation.4 | async-start | bytes 7864320 | tf_op jit(solution)/shard_map/all_gather | solution.py:41
  13.5 97.8 %all-gather.9.cloned.1.call-start = ((), (), s32[]{:S(2)}) async-start(), calls=%async_computation.5 | async-start | bytes 7864320 | tf_op jit(solution)/shard_map/all_gather | solution.py:42
  69.2 6.6 copy-start.1
  69.2 144.4 %all-to-all-start = ((bf16[384,8,1024]{2,0,1:T(8,128)(2,1)}), bf16[384,8,1024]{2,0,1:T(8,128)(2,1)}, u32[]{:S(2)}, u32[]{:S(2)}) async-start(bf16[384,8,1024]{2,0,1:T(8,128)(2,1)} %bitcast.40), calls=%async_computation | async-start | bytes 12582912 | tf_op jit(solution)/shard_map/all_to_all | solution.py:49
  75.0 144.0 %all-gather.13.cloned.1.call-start = ((), (), s32[]{:S(2)}) async-start(), calls=%async_computation.8 | async-start | bytes 7864320 | tf_op jit(solution)/shard_map/all_gather | solution.py:44
  213.7 142.5 %all-to-all-start.1 = ((bf16[384,8,1024]{2,0,1:T(8,128)(2,1)}), bf16[384,8,1024]{2,0,1:T(8,128)(2,1)}, u32[]{:S(2)}, u32[]{:S(2)}) async-start(bf16[384,8,1024]{2,0,1:T(8,128)(2,1)} %bitcast.41), calls=%async_computation.1 | async-start | bytes 12582912 | tf_op jit(solution)/shard_map/all_to_all | solution.py:50
  218.4 146.2 %all-gather.15.cloned.1.call-start = ((), (), s32[]{:S(2)}) async-start(), calls=%async_computation.9 | async-start | bytes 7864320 | tf_op jit(solution)/shard_map/all_gather | solution.py:45
  356.1 163.1 %all-to-all-start.2 = ((bf16[384,8,1024]{2,0,1:T(8,128)(2,1)}), bf16[384,8,1024]{2,0,1:T(8,128)(2,1)}, u32[]{:S(2)}, u32[]{:S(2)}) async-start(bf16[384,8,1024]{2,0,1:T(8,128)(2,1)} %bitcast.39), calls=%async_computation.2 | async-start | bytes 12582912 | tf_op jit(solution)/shard_map/all_to_all | solution.py:51
  361.0 3.4 copy-start
  361.0 50.2 %all-gather.11.cloned.1.call-start = ((), (), s32[]{:S(2)}) async-start(), calls=%async_computation.6 | async-start | bytes 7864320 | tf_op jit(solution)/shard_map/all_gather | solution.py:43
  364.3 294.2 %all-reduce.3.cloned.1.call-start = ((), (), s32[]{:S(2)}) async-start(), calls=%async_computation.7 | async-start | bytes 3145728 | tf_op jit(solution)/shard_map/psum | solution.py:18
  519.3 185.0 %all-to-all-start.3 = ((bf16[384,8,1024]{2,0,1:T(8,128)(2,1)}), bf16[384,8,1024]{2,0,1:T(8,128)(2,1)}, u32[]{:S(2)}, u32[]{:S(2)}) async-start(bf16[384,8,1024]{2,0,1:T(8,128)(2,1)} %bitcast.38), calls=%async_computation.3 | async-start | bytes 12582912 | tf_op jit(solution)/shard_map/all_to_all | solution.py:52
  524.1 136.0 %copy-start.2 = (f32[3072]{0:T(1024)S(1)}, f32[3072]{0:T(1024)}, u32[]{:S(2)}) copy-start(f32[3072]{0:T(1024)} %param.19) | copy-start | bytes 36868
  524.1 180.1 %all-gather.17.cloned.1.call-start = ((), (), s32[]{:S(2)}) async-start(), calls=%async_computation.10 | async-start | bytes 7864320 | tf_op jit(solution)/shard_map/all_gather | solution.py:46
  527.4 273.9 %all-reduce.5.cloned.1.call-start = ((), (), s32[]{:S(2)}) async-start(), calls=%async_computation.11 | async-start | bytes 3145728 | tf_op jit(solution)/shard_map/psum | solution.py:18
  711.9 91.1 %copy-start.3 = (f32[3072]{0:T(1024)S(1)}, f32[3072]{0:T(1024)}, u32[]{:S(2)}) copy-start(f32[3072]{0:T(1024)} %param.21) | copy-start | bytes 36868
  805.6 12.7 %slice-start = ((s8[6291456]{0:T(1024)(128)(4,1)}), s8[4194304]{0:T(1024)(128)(4,1)S(1)}, s32[]{:S(2)}) async-start(s8[6291456]{0:T(1024)(128)(4,1)} %bitcast.34), calls=%async_computation.12 | async-start | bytes 8388608
  812.0 6.4 slice-start.1
  821.0 12.7 %slice-start.2 = ((s8[6291456]{0:T(1024)(128)(4,1)}), s8[4194304]{0:T(1024)(128)(4,1)S(1)}, s32[]{:S(2)}) async-start(s8[6291456]{0:T(1024)(128)(4,1)} %bitcast.36), calls=%async_computation.14 | async-start | bytes 8388608
  827.4 6.4 slice-start.3
Sparse Core Ops, SparseCore 0:
  13.6 49.0 all-gather.6
  64.9 46.3 all-gather.8
  113.4 46.3 all-gather.12
  221.1 46.7 all-gather.14
  364.4 46.6 all-gather.10
  419.0 239.4 all-reduce.2
  660.6 43.5 all-gather.16
  712.1 89.2 all-reduce.4
where the time goes:
time: 844 us; the launch traced here: 843 us
  waiting for transfers between devices  701 us (83%)
  local copies, waits for them, and re-layouts  58.5 us (7%)
  other arithmetic  24.5 us (3%)
  matrix products  24.2 us (3%)
  starting transfers between devices  20.7 us (2%)
  between operations  14.3 us (2%)
    psum x2, waiting for transfers between devices, half_step(): total = lax.psum(partial_value, 'fs')  220 us
    all_to_all x1, waiting for transfers between devices, per_device(): lax.all_to_all(wide[1], 'fs', split_axis=1, concat_axis=0, tiled=True)  131 us
    all_to_all x1, waiting for transfers between devices, per_device(): lax.all_to_all(wide[3], 'fs', split_axis=1, concat_axis=0, tiled=True)  100 us
    all_to_all x1, waiting for transfers between devices, per_device(): lax.all_to_all(wide[0], 'fs', split_axis=1, concat_axis=0, tiled=True)  95.9 us
    all_gather x1, waiting for transfers between devices, per_device(): lax.all_gather((gain_a * gate_first).astype(jnp.bfloat16), 'tp', axis=1,...  48.5 us
    all_gather x1, waiting for transfers between devices, per_device(): lax.all_gather(down_second.astype(jnp.bfloat16), 'tp', axis=1, tiled=True)  38 us
    all_gather x1, waiting for transfers between devices, per_device(): lax.all_gather(down_first.astype(jnp.bfloat16), 'tp', axis=1, tiled=True)  35.5 us
    unnamed x22, local copies, waits for them, and re-layouts  30.9 us
  transfers between devices with their start and end apart: 12, of which 9 were waited for; matrix products, arithmetic and copies ran while one was open for 7% of the time, Pallas kernels for 0%

commit v1 on v0

--- a/solution.py
+++ b/solution.py
@@ -1,9 +1,17 @@
+import functools
 import jax
 import jax.numpy as jnp
 from jax import lax
 from jax.sharding import PartitionSpec as P
 
 EPSILON = 1e-06
+
+
+def _perform_words(matrix, lane_axis):
+    return lax.all_gather(matrix, axis_name=lane_axis).sum(axis=0)
+
+
+map_unit = functools.partial(_perform_words, lane_axis="fs")
 
 
 def half_step(rows, gate, up, down, post_gain):
@@ -15,7 +23,7 @@
     up_pre = jnp.dot(normed, up, preferred_element_type=jnp.float32)
     hidden = (jax.nn.silu(gate_pre) * up_pre).astype(jnp.bfloat16)
     partial_value = jnp.dot(hidden, down, preferred_element_type=jnp.float32)
-    total = lax.psum(partial_value, "fs")
+    total = map_unit(partial_value)
     scale = lax.rsqrt(jnp.mean(total * total, axis=-1, keepdims=True) + EPSILON)
     return (floats + 0.5 * total * scale * post_gain[None, :]).astype(jnp.bfloat16)
 

time: 844 us -> 1030 us (1.22)
  waiting for transfers between devices: 701 us -> 878 us
    psum x2 -> x0, waiting for transfers between devices: 220 us -> none  [half_step(): total = lax.psum(partial_value, 'fs')]
    all_gather x0 -> x2, waiting for transfers between devices: none -> 208 us  [_perform_words(): return lax.all_gather(matrix, axis_name=lane_axis).sum(axis=0)]
    all_to_all x1, waiting for transfers between devices: 100 us -> 264 us  [per_device(): lax.all_to_all(wide[3], 'fs', split_axis=1, concat_axis=0, tiled=True)]
    all_gather x1, waiting for transfers between devices: 35.5 us -> 0.02 us  [per_device(): lax.all_gather(down_first.astype(jnp.bfloat16), 'tp', axis=1, tiled=True)]
    all_gather x1, waiting for transfers between devices: 38 us -> 69.8 us  [per_device(): lax.all_gather(down_second.astype(jnp.bfloat16), 'tp', axis=1, tiled=True)]
    all_to_all x1, waiting for transfers between devices: 0.01 us -> 29.5 us  [per_device(): lax.all_to_all(wide[4], 'fs', split_axis=1, concat_axis=0, tiled=True)]
    reduce_sum x0 -> x2, other arithmetic: none -> 11.9 us  [_perform_words(): return lax.all_gather(matrix, axis_name=lane_axis).sum(axis=0)]
    unnamed x22 -> x24, local copies, waits for them, and re-layouts: 30.9 us -> 31.9 us
  transfers between devices with their start and end apart: 12 -> 12, of which waited for: 9 -> 9; matrix products, arithmetic and copies ran while one was open for 7% -> 6% of each run, Pallas kernels for 0% -> 0%
where the time goes in v1:
time: 1030 us
  waiting for transfers between devices  878 us (85%)
  local copies, waits for them, and re-layouts  59.8 us (6%)
  other arithmetic  28.8 us (3%)
  matrix products  23.1 us (2%)
  starting transfers between devices  20.9 us (2%)
  between operations  14.2 us (1%)
    all_to_all x1, waiting for transfers between devices, per_device(): lax.all_to_all(wide[3], 'fs', split_axis=1, concat_axis=0, tiled=True)  264 us
    all_gather x2, waiting for transfers between devices, _perform_words(): return lax.all_gather(matrix, axis_name=lane_axis).sum(axis=0)  208 us
    all_to_all x1, waiting for transfers between devices, per_device(): lax.all_to_all(wide[1], 'fs', split_axis=1, concat_axis=0, tiled=True)  133 us
    all_to_all x1, waiting for transfers between devices, per_device(): lax.all_to_all(wide[0], 'fs', split_axis=1, concat_axis=0, tiled=True)  95.9 us
    all_gather x1, waiting for transfers between devices, per_device(): lax.all_gather(down_second.astype(jnp.bfloat16), 'tp', axis=1, tiled=True)  69.8 us
    all_gather x1, waiting for transfers between devices, per_device(): lax.all_gather((gain_a * gate_first).astype(jnp.bfloat16), 'tp', axis=1,...  46 us
    unnamed x24, local copies, waits for them, and re-layouts  31.9 us
    all_gather x1, waiting for transfers between devices, per_device(): lax.all_gather((gain_a * up_first).astype(jnp.bfloat16), 'tp', axis=1, ti...  30.9 us
  transfers between devices with their start and end apart: 12, of which 9 were waited for; matrix products, arithmetic and copies ran while one was open for 6% of the time, Pallas kernels for 0%

profile of v1, /device:TPU:0, one launch (start us, length us, event | category | flops | bytes accessed | tf_op | source)
XLA Modules:
  0.0 1025.1 jit_solution(3632938610966043488)
XLA Ops:
  7.2 0.8 dynamic_slice.6
  8.0 5.5 multiply_convert_fusion.3
  13.5 0.0 all-gather.13.cloned.1.call-start
  13.6 0.7 all-gather.13.cloned.1.call-update
  14.3 0.0 all-gather.15.cloned.1.call-start
  14.3 1.1 copy-done.2
  15.4 1.3 convert_element_type.47
  16.7 46.0 %all-gather.11.cloned.1.call-done = bf16[384,8192]{1,0:T(8,128)(2,1)} async-done(((bf16[384,2048]{1,0:T(8,128)(2,1)}), bf16[384,8192]{1,0:T(8,128)(2,1)}) %all-gather.11.cloned.1.call-update) | async-done | bytes 6291472 | tf_op jit(solution)/shard_map/all_gather | solution.py:49
  62.7 6.5 copy.33
  69.2 5.8 all-to-all-start
  75.1 0.8 dynamic_slice.7
  75.8 4.5 multiply_convert_fusion.1
  80.4 30.9 %all-gather.13.cloned.1.call-done = bf16[384,8192]{1,0:T(8,128)(2,1)} async-done(((bf16[384,2048]{1,0:T(8,128)(2,1)}), bf16[384,8192]{1,0:T(8,128)(2,1)}) %all-gather.13.cloned.1.call-update) | async-done | bytes 6291472 | tf_op jit(solution)/shard_map/all_gather | solution.py:50
  111.3 6.5 copy.32
  117.8 95.9 %all-to-all-done = bf16[384,8,1024]{2,0,1:T(8,128)(2,1)} async-done(((bf16[384,8,1024]{2,0,1:T(8,128)(2,1)}), bf16[384,8,1024]{2,0,1:T(8,128)(2,1)}, u32[]{:S(2)}, u32[]{:S(2)}) %all-to-all-start) | async-done | bytes 6291488 | tf_op jit(solution)/shard_map/all_to_all | solution.py:57
  213.7 5.0 all-to-all-start.1
  218.6 0.0 all-gather.19.cloned.1.call-start
  218.7 0.5 all-gather.19.cloned.1.call-update
  219.3 0.2 fusion
  219.5 3.8 fusion.26
  223.4 133.0 %all-to-all-done.1 = bf16[384,8,1024]{2,0,1:T(8,128)(2,1)} async-done(((bf16[384,8,1024]{2,0,1:T(8,128)(2,1)}), bf16[384,8,1024]{2,0,1:T(8,128)(2,1)}, u32[]{:S(2)}, u32[]{:S(2)}) %all-to-all-start.1) | async-done | bytes 6291488 | tf_op jit(solution)/shard_map/all_to_all | solution.py:58
  356.3 7.7 fusion.9
  364.1 6.7 copy.31
  370.9 4.9 all-to-all-start.2
  375.8 6.5 copy.30
  382.3 263.5 %all-to-all-done.2 = bf16[384,8,1024]{2,0,1:T(8,128)(2,1)} async-done(((bf16[384,8,1024]{2,0,1:T(8,128)(2,1)}), bf16[384,8,1024]{2,0,1:T(8,128)(2,1)}, u32[]{:S(2)}, u32[]{:S(2)}) %all-to-all-start.2) | async-done | bytes 6291488 | tf_op jit(solution)/shard_map/all_to_all | solution.py:59
  645.9 4.8 all-to-all-start.3
  650.6 0.0 all-gather.21.cloned.1.call-start
  650.7 3.2 convert_element_type.54
  653.9 0.2 all-gather.25.cloned.1.call-start
  654.1 33.6 %all-gather.23.cloned.1.call-done = f32[1024,3072]{1,0:T(8,128)} async-done(((f32[128,3072]{1,0:T(8,128)}), f32[1024,3072]{1,0:T(8,128)}) %all-gather.23.cloned.1.call-update) | async-done | bytes 12582928 | tf_op jit(solution)/shard_map/all_gather | solution.py:11
  687.7 6.0 reduce_sum.55
  693.7 0.2 multiply_reduce_fusion.1
  693.9 0.5 fusion.3
  694.4 3.8 fusion.22
  698.2 69.8 %all-gather.21.cloned.1.call-done = bf16[1024,3072]{1,0:T(8,128)(2,1)} async-done(((bf16[1024,768]{1,0:T(8,128)(2,1)}), bf16[1024,3072]{1,0:T(8,128)(2,1)}) %all-gather.21.cloned.1.call-update) | async-done | bytes 6291472 | tf_op jit(solution)/shard_map/all_gather | solution.py:54
  768.1 29.5 %all-to-all-done.3 = bf16[384,8,1024]{2,0,1:T(8,128)(2,1)} async-done(((bf16[384,8,1024]{2,0,1:T(8,128)(2,1)}), bf16[384,8,1024]{2,0,1:T(8,128)(2,1)}, u32[]{:S(2)}, u32[]{:S(2)}) %all-to-all-start.3) | async-done | bytes 6291488 | tf_op jit(solution)/shard_map/all_to_all | solution.py:60
  797.6 7.7 fusion.8
  805.3 174.7 %all-gather.25.cloned.1.call-done = f32[1024,3072]{1,0:T(8,128)} async-done(((f32[128,3072]{1,0:T(8,128)}), f32[1024,3072]{1,0:T(8,128)}) %all-gather.25.cloned.1.call-update) | async-done | bytes 12582928 | tf_op jit(solution)/shard_map/all_gather | solution.py:11
  980.0 6.0 reduce_sum.58
  986.0 0.2 multiply_reduce_fusion
  986.2 1.2 fusion.5
  987.4 6.4 copy.40
  993.8 6.3 copy.41
  1000.1 2.7 copy.42
  1002.8 6.4 copy.43
  1009.2 6.3 copy.44
  1015.6 2.7 copy.45
  (35 shorter events, 0.3 us)
Async XLA Ops:
  7.2 55.6 %all-gather.11.cloned.1.call-start = ((), (), s32[]{:S(2)}) async-start(), calls=%async_computation.4 | async-start | bytes 7864320 | tf_op jit(solution)/shard_map/all_gather | solution.py:49
  13.5 1.9 copy-start.2
  13.5 97.8 %all-gather.13.cloned.1.call-start = ((), (), s32[]{:S(2)}) async-start(), calls=%async_computation.5 | async-start | bytes 7864320 | tf_op jit(solution)/shard_map/all_gather | solution.py:50
  14.3 209.1 %all-gather.15.cloned.1.call-start = ((), (), s32[]{:S(2)}) async-start(), calls=%async_computation.6 | async-start | bytes 7864320 | tf_op jit(solution)/shard_map/all_gather | solution.py:51
  69.2 6.6 copy-start.1
  69.2 144.4 %all-to-all-start = ((bf16[384,8,1024]{2,0,1:T(8,128)(2,1)}), bf16[384,8,1024]{2,0,1:T(8,128)(2,1)}, u32[]{:S(2)}, u32[]{:S(2)}) async-start(bf16[384,8,1024]{2,0,1:T(8,128)(2,1)} %bitcast.42), calls=%async_computation | async-start | bytes 12582912 | tf_op jit(solution)/shard_map/all_to_all | solution.py:57
  75.0 289.1 %all-gather.17.cloned.1.call-start = ((), (), s32[]{:S(2)}) async-start(), calls=%async_computation.7 | async-start | bytes 7864320 | tf_op jit(solution)/shard_map/all_gather | solution.py:52
  213.7 5.6 copy-start
  213.7 142.7 %all-to-all-start.1 = ((bf16[384,8,1024]{2,0,1:T(8,128)(2,1)}), bf16[384,8,1024]{2,0,1:T(8,128)(2,1)}, u32[]{:S(2)}, u32[]{:S(2)}) async-start(bf16[384,8,1024]{2,0,1:T(8,128)(2,1)} %bitcast.41), calls=%async_computation.1 | async-start | bytes 12582912 | tf_op jit(solution)/shard_map/all_to_all | solution.py:58
  218.6 157.2 %all-gather.19.cloned.1.call-start = ((), (), s32[]{:S(2)}) async-start(), calls=%async_computation.8 | async-start | bytes 7864320 | tf_op jit(solution)/shard_map/all_gather | solution.py:53
  219.2 468.5 %all-gather.23.cloned.1.call-start = ((), (), s32[]{:S(2)}) async-start(), calls=%async_computation.10 | async-start | bytes 14155776 | tf_op jit(solution)/shard_map/all_gather | solution.py:11
  370.9 275.0 %all-to-all-start.2 = ((bf16[384,8,1024]{2,0,1:T(8,128)(2,1)}), bf16[384,8,1024]{2,0,1:T(8,128)(2,1)}, u32[]{:S(2)}, u32[]{:S(2)}) async-start(bf16[384,8,1024]{2,0,1:T(8,128)(2,1)} %bitcast.43), calls=%async_computation.2 | async-start | bytes 12582912 | tf_op jit(solution)/shard_map/all_to_all | solution.py:59
  645.9 151.7 %all-to-all-start.3 = ((bf16[384,8,1024]{2,0,1:T(8,128)(2,1)}), bf16[384,8,1024]{2,0,1:T(8,128)(2,1)}, u32[]{:S(2)}, u32[]{:S(2)}) async-start(bf16[384,8,1024]{2,0,1:T(8,128)(2,1)} %bitcast.40), calls=%async_computation.3 | async-start | bytes 12582912 | tf_op jit(solution)/shard_map/all_to_all | solution.py:60
  650.6 117.4 %all-gather.21.cloned.1.call-start = ((), (), s32[]{:S(2)}) async-start(), calls=%async_computation.9 | async-start | bytes 7864320 | tf_op jit(solution)/shard_map/all_gather | solution.py:54
  653.9 326.1 %all-gather.25.cloned.1.call-start = ((), (), s32[]{:S(2)}) async-start(), calls=%async_computation.11 | async-start | bytes 14155776 | tf_op jit(solution)/shard_map/all_gather | solution.py:11
  687.7 6.2 copy-start.3
  980.0 6.2 copy-start.4
  987.4 12.7 %slice-start = ((s8[6291456]{0:T(1024)(128)(4,1)}), s8[4194304]{0:T(1024)(128)(4,1)S(1)}, s32[]{:S(2)}) async-start(s8[6291456]{0:T(1024)(128)(4,1)} %bitcast.36), calls=%async_computation.12 | async-start | bytes 8388608
  993.8 6.4 slice-start.1
  1002.8 12.7 %slice-start.2 = ((s8[6291456]{0:T(1024)(128)(4,1)}), s8[4194304]{0:T(1024)(128)(4,1)S(1)}, s32[]{:S(2)}) async-start(s8[6291456]{0:T(1024)(128)(4,1)} %bitcast.38), calls=%async_computation.14 | async-start | bytes 8388608
  1009.2 6.4 slice-start.3
Sparse Core Ops, SparseCore 0:
  13.6 49.0 all-gather.10
  64.9 46.3 all-gather.12
  113.4 46.3 all-gather.14
  161.8 46.3 all-gather.16
  221.3 46.7 all-gather.18
  364.2 323.4 all-gather.22
  689.9 78.1 all-gather.20
  805.4 174.5 all-gather.24
